TPU v7x, 256 devices: a whole 4x4x8 slice. The times are simulated.
256 devices in a mesh: sp: 16 (over y, x), tp: 16 (over z, core).
Axes of the slice: x: 4, y: 4, z: 8, core: 2. Of those that a mesh axis runs over, the one named last changes fastest.
Arguments:
- stream: bfloat16 [2048, 16384], P('tp', 'sp'), may hold values from -12 to 12
- norm_gain: float32 [2, 2048], P(None, 'tp'), may hold values from 0.1 to 1.9
- in_weight: bfloat16 [2, 2048, 1024], P(None, 'sp', 'tp'), may hold values from -0.125 to 0.125
- out_weight: bfloat16 [2, 1024, 2048], P(None, 'tp', 'sp'), may hold values from -0.1875 to 0.1875
- docs: int32 [16384], P('sp'), may hold values from 0 to 3, never falling along the last dimension, each value on 1 to 8192 neighbouring positions
Outputs:
- mixed_out: bfloat16 [2048, 16384], P('tp', 'sp')
Inputs may be any that keep to these rules, and one draw needn't show every extreme that they name: `docs`: numbers never fall along the positions and start at 0; a document spans at most 8192 positions.
All inputs are finite; a program needn't handle non-finite values.
Results may differ from a plain program's by a relative error of at most 0.0095.
Values may be sent and summed in bfloat16 or wider, within the bound.
A program may use at most 64 MiB of HBM per device.

v0:
```python
import jax
import jax.numpy as jnp
from jax import lax
from jax.sharding import Mesh
from jax.sharding import PartitionSpec as P

D = 2048
PW = 1024
GROUPS = 4
WIDEST = 16
LAYERS = 2
TP = ("tp_0", "tp_1")


contract_rows = (((0,), (0,)), ((), ()))


def rows_first(arrays, axis, dims):
    turned = [jnp.moveaxis(a, dim, 0) for a, dim in zip(arrays, dims)]
    widths = [t[0].size for t in turned]
    both = jnp.concatenate([t.reshape(-1, w) for t, w in zip(turned, widths)], axis=1)
    result = lax.all_gather(both, axis, axis=0, tiled=True)
    blocks = jnp.split(result, [sum(widths[:k]) for k in range(1, len(widths))], axis=1)
    return tuple(
        (
            jnp.moveaxis(b.reshape(-1, *t.shape[1:]), 0, dim)
            for b, t, dim in zip(blocks, turned, dims)
        )
    )


def sent_to_all(array, axis):
    copies = jnp.broadcast_to(array, (lax.axis_size(axis), *array.shape))
    return lax.all_to_all(copies, axis, split_axis=0, concat_axis=0, tiled=True)


def taken_together(array, axis):
    return sent_to_all(array, axis).sum(axis=0)


def passed_along(block, axis, distance):
    devices = range(lax.axis_size(axis))
    route = [(i - distance, i) for i in devices if i - distance in devices]
    return lax.ppermute(block, axis, route)


def whole_of(array, axes, dim):
    for axis in reversed(axes):
        array = lax.all_gather(array, axis, axis=dim, tiled=True)
    return array


def trailing_pool(values, docs_own, edge_values, edge_docs, widths):
    length = values.shape[1]
    reach_back = WIDEST - 1
    extended = jnp.concatenate([edge_values, values], axis=1).astype(jnp.float32)
    ext_docs = jnp.concatenate([edge_docs, docs_own + 1])
    marker = docs_own + 1
    window_sum = jnp.zeros(values.shape, jnp.float32)
    members = jnp.zeros(values.shape, jnp.float32)
    for lag_step in range(WIDEST):
        lower_edge = reach_back - lag_step
        shifted = lax.slice_in_dim(extended, lower_edge, lower_edge + length, axis=1)
        same_doc = lax.slice_in_dim(ext_docs, lower_edge, lower_edge + length) == marker
        inside = jnp.logical_and(same_doc[None, :], lag_step < widths[:, None])
        window_sum = window_sum + jnp.where(inside, shifted, jnp.float32(0.0))
        members = members + inside.astype(jnp.float32)
    return (window_sum / members - values.astype(jnp.float32)).astype(jnp.bfloat16)


def per_device(stream, norm_gain, in_weight, out_weight, docs):
    local_rows, length = stream.shape
    pool_rows = in_weight.shape[2]
    channel = lax.axis_index(TP) * pool_rows + lax.iota(jnp.int32, pool_rows)
    widths = jnp.left_shift(jnp.int32(2), channel // (PW // GROUPS))
    residual = stream.astype(jnp.float32)
    for layer_idx in range(LAYERS):
        in_block, out_rows = rows_first((in_weight[layer_idx], out_weight[layer_idx]), "sp", (0, 1))
        squares = taken_together(jnp.sum(residual * residual, axis=0), TP)
        scaled = residual * lax.rsqrt(squares / D + 1e-06)[None, :] * norm_gain[layer_idx][:, None]
        normed = scaled.astype(jnp.bfloat16)
        pool_in = lax.dot_general(
            in_block,
            lax.all_gather(normed, TP, axis=0, tiled=True),
            contract_rows,
            preferred_element_type=jnp.float32,
        ).astype(jnp.bfloat16)
        tail_from = length - WIDEST + 1
        edge_values, edge_docs = passed_along(
            (pool_in[:, tail_from:], docs[tail_from:] + 1), "sp", 1
        )
        pooled = trailing_pool(pool_in, docs, edge_values, edge_docs, widths)
        out_cols = lax.all_to_all(out_rows, TP, split_axis=1, concat_axis=0, tiled=True)
        change = lax.dot_general(
            out_cols, whole_of(pooled, TP, 0), contract_rows, preferred_element_type=jnp.float32
        )
        residual = residual + change
    return residual.astype(jnp.bfloat16)


def solution(mesh):
    finer = Mesh(mesh.devices.reshape(mesh.shape["sp"], 8, 2), ("sp", "tp_0", "tp_1"))
    return jax.shard_map(
        per_device,
        mesh=finer,
        in_specs=(P(TP, "sp"), P(None, TP), P(None, "sp", TP), P(None, TP, "sp"), P("sp")),
        out_specs=P(TP, "sp"),
        check_vma=False,
    )
```

profile of v0, /device:TPU:8, one launch (start us, length us, event | category | flops | bytes accessed | tf_op | source)
XLA Modules:
  0.0 235.5 jit_solution(13317985873692921568)
XLA Ops:
  6.5 1.0 fusion.1
  7.6 0.7 broadcast_in_dim.39
  8.2 8.6 %all-to-all-start.1 = ((f32[16,1,1024]{2,1,0:T(1,128)}), f32[16,1,1024]{2,1,0:T(1,128)S(1)}, u32[]{:S(2)}, u32[]{:S(2)}) async-start(f32[16,1,1024]{2,1,0:T(1,128)} %broadcast_in_dim.39), calls=%async_computation.1 | async-start | bytes 131072 | tf_op jit(solution)/shard_map/all_to_all | solution.py:34
  16.8 0.0 all-gather.5.cloned.1.call-start
  16.8 0.8 slice_bitcast_fusion.6
  17.6 7.0 %all-to-all-done.1 = f32[16,1,1024]{2,1,0:T(1,128)S(1)} async-done(((f32[16,1,1024]{2,1,0:T(1,128)}), f32[16,1,1024]{2,1,0:T(1,128)S(1)}, u32[]{:S(2)}, u32[]{:S(2)}) %all-to-all-start.1) | async-done | bytes 65568 | tf_op jit(solution)/shard_map/all_to_all | solution.py:34
  24.6 0.1 reduce_sum.37
  24.7 1.8 fusion.3
  26.4 0.0 all-gather.5.cloned.1.call-update
  26.4 0.0 all-gather.7.cloned.1.call-start
  26.5 0.8 slice_add_fusion
  27.2 3.4 %collective-permute-start.1 = (s32[15]{0:T(128)S(1)}, s32[15]{0:T(128)S(1)}, u32[]{:S(2)}, u32[]{:S(2)}) collective-permute-start(s32[15]{0:T(128)S(1)} %slice_add_fusion), channel_id=1, source_target_pairs={{0,16},{16,32},{32,48},{48,64},{64,80},{80,96},{96,112},{112,128},... | collective-permute-start | bytes 188 | tf_op jit(solution)/shard_map/ppermute | solution.py:44
  30.8 0.7 slice_bitcast_fusion.3
  31.5 0.7 slice_bitcast_fusion.2
  32.3 24.6 %all_gather.24 = bf16[2048,128]{0,1:T(8,128)(2,1)S(1)} all-gather(bf16[128,128]{0,1:T(8,128)(2,1)S(1)} %pad_maximum_fusion), channel_id=1, replica_groups=mesh['sp'=16,'tp_0'=8,'tp_1'=2] {'sp'}, dimensions={0}, use_global_device_ids=true | all-gather | bytes 557056 | tf_op jit(solution)/shard_map/all_gather | solution.py:22
  56.9 0.7 broadcast_add_fusion
  57.6 0.0 collective-permute-done.1
  57.6 0.1 fusion.56
  57.7 7.6 %all-gather.5.cloned.1.call-done = bf16[2048,1024]{1,0:T(8,128)(2,1)} async-done(((bf16[128,1024]{1,0:T(8,128)(2,1)}), bf16[2048,1024]{1,0:T(8,128)(2,1)}) %all-gather.5.cloned.1.call-update) | async-done | bytes 4194320 | tf_op jit(solution)/shard_map/all_gather | solution.py:84
  65.3 3.0 %convolution_convert_fusion.1 = bf16[64,1024]{1,0:T(8,128)(2,1)S(1)} fusion(bf16[2048,1024]{1,0:T(8,128)(2,1)} %all-gather.5.cloned.1.call-done, bf16[2048,128]{0,1:T(8,128)(2,1)S(1)} %all_gather.24), kind=kOutput, calls=%fused_computation.4 | convolution fusion | flops 268500992 | bytes 4587520 | tf_op jit(solution)/shard_map/dot_general | solution.py:82
  68.3 0.0 copy-start
  68.3 0.1 slice.240
  68.4 3.4 %collective-permute-start = (bf16[64,15]{1,0:T(8,128)(2,1)S(1)}, bf16[64,15]{1,0:T(8,128)(2,1)S(1)}, u32[]{:S(2)}, u32[]{:S(2)}) collective-permute-start(bf16[64,15]{1,0:T(8,128)(2,1)S(1)} %slice.240), channel_id=1, source_target_pairs={{0,16},{16,32},{32,48},{48,64},{64,80},{80,96},{96,112},{112,128},... | collective-permute-start | bytes 5768 | tf_op jit(solution)/shard_map/ppermute | solution.py:44
  71.8 0.1 fusion.58
  71.9 4.2 %collective-permute-done = bf16[64,15]{1,0:T(8,128)(2,1)S(1)} collective-permute-done((bf16[64,15]{1,0:T(8,128)(2,1)S(1)}, bf16[64,15]{1,0:T(8,128)(2,1)S(1)}, u32[]{:S(2)}, u32[]{:S(2)}) %collective-permute-start) | collective-permute-done | bytes 1952 | tf_op jit(solution)/shard_map/ppermute | solution.py:44
  76.2 0.1 maximum_convert_fusion
  76.3 1.4 subtract_convert_fusion.1
  77.6 2.1 all_gather.26
  79.8 0.0 all-gather.7.cloned.1.call-update
  79.8 0.0 all-gather.9.cloned.1.call-start
  79.8 0.1 copy_bitcast_fusion.1
  79.9 16.2 %all_to_all.50 = bf16[64,16,128]{2,0,1:T(8,128)(2,1)S(1)} all-to-all(bf16[64,16,128]{2,0,1:T(8,128)(2,1)S(1)} %copy_bitcast_fusion.1), channel_id=1, replica_groups=mesh['sp'=16,'tp_0'=8,'tp_1'=2] {'tp_0','tp_1'}, dimensions={1} | all-to-all | bytes 524288 | tf_op jit(solution)/shard_map/all_to_all | solution.py:93
  96.0 23.6 %all-gather.7.cloned.1.call-done = bf16[1024,1024]{1,0:T(8,128)(2,1)} async-done(((bf16[128,1024]{1,0:T(8,128)(2,1)}), bf16[1024,1024]{1,0:T(8,128)(2,1)}) %all-gather.7.cloned.1.call-update) | async-done | bytes 2097168 | tf_op jit(solution)/shard_map/all_gather | solution.py:49
  119.7 0.0 copy-done
  119.7 2.1 multiply_reduce_fusion
  121.8 12.2 %all_to_all.51 = f32[16,1,1024]{2,1,0:T(1,128)S(1)} all-to-all(f32[16,1,1024]{2,1,0:T(1,128)S(1)} %broadcast_in_dim.41), channel_id=1, replica_groups=mesh['sp'=16,'tp_0'=8,'tp_1'=2] {'tp_0','tp_1'}, dimensions={0} | all-to-all | bytes 131072 | tf_op jit(solution)/shard_map/all_to_all | solution.py:34
  134.0 0.1 reduce_sum.39
  134.0 0.8 multiply_convert_fusion
  134.8 0.0 all-gather.9.cloned.1.call-update
  134.8 0.0 all-gather.11.cloned.1.call-start
  134.9 23.4 %all_gather.28 = bf16[2048,128]{0,1:T(8,128)(2,1)S(1)} all-gather(bf16[128,128]{0,1:T(8,128)(2,1)S(1)} %pad_maximum_fusion.1), channel_id=1, replica_groups=mesh['sp'=16,'tp_0'=8,'tp_1'=2] {'sp'}, dimensions={0}, use_global_device_ids=true | all-gather | bytes 557056 | tf_op jit(solution)/shard_map/all_gather | solution.py:22
  158.3 13.6 %all-gather.9.cloned.1.call-done = bf16[2048,1024]{1,0:T(8,128)(2,1)} async-done(((bf16[128,1024]{1,0:T(8,128)(2,1)}), bf16[2048,1024]{1,0:T(8,128)(2,1)}) %all-gather.9.cloned.1.call-update) | async-done | bytes 4194320 | tf_op jit(solution)/shard_map/all_gather | solution.py:84
  171.9 3.0 %convolution_convert_fusion = bf16[64,1024]{1,0:T(8,128)(2,1)S(1)} fusion(bf16[2048,1024]{1,0:T(8,128)(2,1)} %all-gather.9.cloned.1.call-done, bf16[2048,128]{0,1:T(8,128)(2,1)S(1)} %all_gather.28), kind=kOutput, calls=%fused_computation.3 | convolution fusion | flops 268500992 | bytes 4587520 | tf_op jit(solution)/shard_map/dot_general | solution.py:82
  175.0 0.1 slice.285
  175.1 3.5 %collective-permute-start.2 = (bf16[64,15]{1,0:T(8,128)(2,1)S(1)}, bf16[64,15]{1,0:T(8,128)(2,1)S(1)}, u32[]{:S(2)}, u32[]{:S(2)}) collective-permute-start(bf16[64,15]{1,0:T(8,128)(2,1)S(1)} %slice.285), channel_id=1, source_target_pairs={{0,16},{16,32},{32,48},{48,64},{64,80},{80,96},{96,112},{112,128},... | collective-permute-start | bytes 5768 | tf_op jit(solution)/shard_map/ppermute | solution.py:44
  178.5 4.2 %collective-permute-done.2 = bf16[64,15]{1,0:T(8,128)(2,1)S(1)} collective-permute-done((bf16[64,15]{1,0:T(8,128)(2,1)S(1)}, bf16[64,15]{1,0:T(8,128)(2,1)S(1)}, u32[]{:S(2)}, u32[]{:S(2)}) %collective-permute-start.2) | collective-permute-done | bytes 1952 | tf_op jit(solution)/shard_map/ppermute | solution.py:44
  182.8 0.1 maximum_convert_fusion.1
  182.9 1.4 subtract_convert_fusion
  184.3 2.1 all_gather.30
  186.4 0.0 all-gather.11.cloned.1.call-update
  186.4 0.1 copy_bitcast_fusion
  186.5 16.2 %all_to_all.52 = bf16[64,16,128]{2,0,1:T(8,128)(2,1)S(1)} all-to-all(bf16[64,16,128]{2,0,1:T(8,128)(2,1)S(1)} %copy_bitcast_fusion), channel_id=1, replica_groups=mesh['sp'=16,'tp_0'=8,'tp_1'=2] {'tp_0','tp_1'}, dimensions={1} | all-to-all | bytes 524288 | tf_op jit(solution)/shard_map/all_to_all | solution.py:93
  202.7 23.5 %all-gather.11.cloned.1.call-done = bf16[1024,1024]{1,0:T(8,128)(2,1)} async-done(((bf16[128,1024]{1,0:T(8,128)(2,1)}), bf16[1024,1024]{1,0:T(8,128)(2,1)}) %all-gather.11.cloned.1.call-update) | async-done | bytes 2097168 | tf_op jit(solution)/shard_map/all_gather | solution.py:49
  226.2 2.8 %fusion = bf16[128,1024]{1,0:T(8,128)(2,1)} fusion(f32[128,1024]{1,0:T(8,128)S(1)} %get-tuple-element.27, bf16[1024,128]{1,0:T(8,128)(2,1)S(1)} %bitcast.41, bf16[1024,1024]{1,0:T(8,128)(2,1)} %all-gather.11.cloned.1.call-done), kind=kOutput, calls=%fused_computation.2 | convolution fusion | flops 268697600 | bytes 3145728 | tf_op jit(solution)/shard_map/dot_general | solution.py:94
  (14 shorter events, 0.2 us)
Async XLA Ops:
  8.2 16.4 %all-to-all-start.1 = ((f32[16,1,1024]{2,1,0:T(1,128)}), f32[16,1,1024]{2,1,0:T(1,128)S(1)}, u32[]{:S(2)}, u32[]{:S(2)}) async-start(f32[16,1,1024]{2,1,0:T(1,128)} %broadcast_in_dim.39), calls=%async_computation.1 | async-start | bytes 131072 | tf_op jit(solution)/shard_map/all_to_all | solution.py:34
  16.8 48.5 %all-gather.5.cloned.1.call-start = ((), (), s32[]{:S(2)}) async-start(), calls=%async_computation.4 | async-start | bytes 4456448 | tf_op jit(solution)/shard_map/all_gather | solution.py:84
  26.4 93.2 %all-gather.7.cloned.1.call-start = ((), (), s32[]{:S(2)}) async-start(), calls=%async_computation.5 | async-start | bytes 2359296 | tf_op jit(solution)/shard_map/all_gather | solution.py:49
  27.2 30.4 %collective-permute-start.1 = (s32[15]{0:T(128)S(1)}, s32[15]{0:T(128)S(1)}, u32[]{:S(2)}, u32[]{:S(2)}) collective-permute-start(s32[15]{0:T(128)S(1)} %slice_add_fusion), channel_id=1, source_target_pairs={{0,16},{16,32},{32,48},{48,64},{64,80},{80,96},{96,112},{112,128},... | collective-permute-start | bytes 188 | tf_op jit(solution)/shard_map/ppermute | solution.py:44
  68.3 51.3 %copy-start = (bf16[128,1024]{1,0:T(8,128)(2,1)S(1)}, bf16[128,1024]{1,0:T(8,128)(2,1)}, u32[]{:S(2)}) copy-start(bf16[128,1024]{1,0:T(8,128)(2,1)} %param.5) | copy-start | bytes 786436
  68.4 7.7 %collective-permute-start = (bf16[64,15]{1,0:T(8,128)(2,1)S(1)}, bf16[64,15]{1,0:T(8,128)(2,1)S(1)}, u32[]{:S(2)}, u32[]{:S(2)}) collective-permute-start(bf16[64,15]{1,0:T(8,128)(2,1)S(1)} %slice.240), channel_id=1, source_target_pairs={{0,16},{16,32},{32,48},{48,64},{64,80},{80,96},{96,112},{112,128},... | collective-permute-start | bytes 5768 | tf_op jit(solution)/shard_map/ppermute | solution.py:44
  79.8 92.2 %all-gather.9.cloned.1.call-start = ((), (), s32[]{:S(2)}) async-start(), calls=%async_computation.6 | async-start | bytes 4456448 | tf_op jit(solution)/shard_map/all_gather | solution.py:84
  134.8 91.4 %all-gather.11.cloned.1.call-start = ((), (), s32[]{:S(2)}) async-start(), calls=%async_computation.7 | async-start | bytes 2359296 | tf_op jit(solution)/shard_map/all_gather | solution.py:49
  175.1 7.7 %collective-permute-start.2 = (bf16[64,15]{1,0:T(8,128)(2,1)S(1)}, bf16[64,15]{1,0:T(8,128)(2,1)S(1)}, u32[]{:S(2)}, u32[]{:S(2)}) collective-permute-start(bf16[64,15]{1,0:T(8,128)(2,1)S(1)} %slice.285), channel_id=1, source_target_pairs={{0,16},{16,32},{32,48},{48,64},{64,80},{80,96},{96,112},{112,128},... | collective-permute-start | bytes 5768 | tf_op jit(solution)/shard_map/ppermute | solution.py:44
Sparse Core Ops, SparseCore 0:
  26.6 38.7 all-gather.4
  79.9 39.7 all-gather.6
  135.0 36.9 all-gather.8
  186.5 39.6 all-gather.10
where the time goes:
time: 236 us
  blocking collectives  96.8 us (41%)
  waiting for transfers between devices  83.9 us (36%)
  starting transfers between devices  19 us (8%)
  between operations  13.3 us (6%)
  matrix products  10.9 us (5%)
  other arithmetic  8.37 us (4%)
  local copies, waits for them, and re-layouts  3.22 us (1%)
    all_gather x2, blocking collectives, rows_first(): result = lax.all_gather(both, axis, axis=0, tiled=True)  48 us
    all_gather x2, waiting for transfers between devices, whole_of(): array = lax.all_gather(array, axis, axis=dim, tiled=True)  47.1 us
    all_to_all x2, blocking collectives, per_device(): lax.all_to_all(out_rows, TP, split_axis=1, concat_axis=0, tiled=True)  32.4 us
    all_gather x2, waiting for transfers between devices, per_device(): lax.all_gather(normed, TP, axis=0, tiled=True)  21.2 us
    all_to_all x1, blocking collectives, sent_to_all(): return lax.all_to_all(copies, axis, split_axis=0, concat_axis=0, tiled=True)  12.2 us
    ppermute x3, starting transfers between devices, passed_along(): return lax.ppermute(block, axis, route)  10.3 us
    all_to_all x1, starting transfers between devices, sent_to_all(): return lax.all_to_all(copies, axis, split_axis=0, concat_axis=0, tiled=True)  8.57 us
    ppermute x3, waiting for transfers between devices, passed_along(): return lax.ppermute(block, axis, route)  8.48 us
  transfers between devices with their start and end apart: 8, of which 7 were waited for; matrix products, arithmetic and copies ran while one was open for 2% of the time, Pallas kernels for 0%

commit v1 on v0

v1 whole, which is shorter than its diff:
```python
import jax
import jax.numpy as jnp
from jax import lax
from jax.experimental import pallas as pl
from jax.experimental.pallas import tpu as pltpu
from jax.sharding import PartitionSpec as P

D = 2048
PW = 1024
LAYERS = 2
NY, NX, NZ = 4, 4, 8
TOK = 128
HALO = 32
ROWS = TOK + HALO
LANES = 128
WAVES = 4
HALF = 32

MESH = pl.DeviceIdType.MESH
NT = (((1,), (1,)), ((), ()))
NN = (((1,), (0,)), ((), ()))

STEP_OFFSETS = ((0,), (-1, 1), (-2, 2), (-3, 3), (4,))


def kernel(
    stream,
    gain,
    in_w,
    out_w,
    docs,
    out,
    weights,
    turned,
    taken,
    gains,
    own_gain,
    edge_docs,
    residual,
    sums_out,
    sums_in,
    last_out,
    last_in,
    mixed,
    masks,
    counts,
    plane_send,
    plane_recv,
    z_send,
    z_recv,
    line_send,
    line_recv,
    far_recv,
    take_send,
    take_recv,
    gain_send,
    gain_recv,
    edge_send,
    edge_recv,
    pair_send,
    pair_recv,
    sums_send,
    sums_recv,
    last_send,
    last_recv,
    mixed_send,
    mixed_recv,
):
    sp = lax.axis_index("sp")
    tp = lax.axis_index("tp")
    y, x = sp // NX, sp % NX
    z, core = tp // 2, tp % 2

    def at(yy, xx, zz):
        return (yy * NX + xx, zz * 2 + core)

    def turn(value, by, size):
        return (value + by + size) % size

    sibling = (sp, z * 2 + 1 - core)
    has_next = jnp.logical_and(z == NZ - 1, sp < NY * NX - 1)
    has_edge = jnp.logical_and(z == 0, sp > 0)

    def copy(src, dst, send, recv, device):
        return pltpu.make_async_remote_copy(
            src_ref=src, dst_ref=dst, send_sem=send, recv_sem=recv, device_id=device, device_id_type=MESH
        )

    def drain(ref, sem):
        pltpu.make_async_copy(ref, ref, sem).wait()

    barrier = pltpu.get_barrier_semaphore()
    peers = [at(turn(y, d, NY), x, z) for d in range(1, NY)]
    peers += [at(y, turn(x, d, NX), z) for d in range(1, NX)]
    peers += [at(y, x, turn(z, d, NZ)) for d in range(1, NZ)]
    peers += [sibling]
    for peer in peers:
        pl.semaphore_signal(barrier, inc=1, device_id=peer, device_id_type=MESH)

    @pl.when(has_next)
    def _():
        pl.semaphore_signal(barrier, inc=1, device_id=(sp + 1, core), device_id_type=MESH)

    @pl.when(has_edge)
    def _():
        pl.semaphore_signal(
            barrier, inc=1, device_id=(sp - 1, (NZ - 1) * 2 + core), device_id_type=MESH
        )

    for layer in range(LAYERS):
        weights[2 * layer, y, x, z] = in_w[layer].astype(jnp.float32).T.astype(jnp.bfloat16)
        weights[2 * layer + 1, y, x, z] = out_w[layer]
    for j in range(NZ):
        block = stream[:, j * TOK : (j + 1) * TOK].astype(jnp.float32)
        turned[j * TOK : (j + 1) * TOK, :] = block.T.astype(jnp.bfloat16)
    own_gain[...] = jnp.zeros_like(own_gain)
    own_gain[0:LAYERS, :] = gain[...]

    extra = jnp.logical_or(has_next, has_edge).astype(jnp.int32)
    pl.semaphore_wait(barrier, len(peers) + extra)

    for d in range(1, NY):
        part = weights.at[:, y, x, z, 0:HALF, :]
        copy(part, part, plane_send, plane_recv, at(turn(y, d, NY), x, z)).start()
    for d in range(1, NX):
        part = weights.at[:, y, x, z, HALF : 2 * HALF, :]
        copy(part, part, plane_send, plane_recv, at(y, turn(x, d, NX), z)).start()

    def slab_a(w, xx, zz):
        return weights.at[w, :, xx, zz, 0:HALF, :]

    def slab_b(w, yy, zz):
        return weights.at[w, yy, :, zz, HALF : 2 * HALF, :]

    def send_z(w, step):
        up, down = at(y, x, turn(z, 1, NZ)), at(y, x, turn(z, -1, NZ))
        before, after = turn(z, -step, NZ), turn(z, step, NZ)
        send, recv = z_send.at[w], z_recv.at[w, step]
        a, b = slab_a(w, x, before), slab_b(w, y, after)
        copy(a, a, send, recv, up).start()
        copy(b, b, send, recv, down).start()
        if step < 3:
            a, b = slab_a(w, x, after), slab_b(w, y, before)
            copy(a, a, send, recv, down).start()
            copy(b, b, send, recv, up).start()

    def wait_z(w, step):
        drain(weights.at[w, 0, 0, 0 : (8 if step < 4 else 4)], z_recv.at[w, step - 1])

    def send_line(w, step):
        for offset in STEP_OFFSETS[step]:
            zz = turn(z, offset, NZ)
            a, b = slab_a(w, x, zz), slab_b(w, y, zz)
            for side in (1, -1):
                copy(a, a, line_send.at[w], line_recv.at[w, step], at(y, turn(x, side, NX), z)).start()
                copy(b, b, line_send.at[w], line_recv.at[w, step], at(turn(y, side, NY), x, z)).start()

    def pass_on(w, step):
        drain(weights.at[w, 0, 0 : len(STEP_OFFSETS[step])], line_recv.at[w, step])
        for offset in STEP_OFFSETS[step]:
            zz = turn(z, offset, NZ)
            ahead = 1 - 2 * (zz % 2)
            a, b = slab_a(w, turn(x, -ahead, NX), zz), slab_b(w, turn(y, -ahead, NY), zz)
            copy(a, a, line_send.at[w], far_recv.at[w], at(y, turn(x, ahead, NX), z)).start()
            copy(b, b, line_send.at[w], far_recv.at[w], at(turn(y, ahead, NY), x, z)).start()

    def wait_far(w):
        drain(weights.at[w, 0], far_recv.at[w])

    def send_taken(d):
        zz = turn(z, d, NZ)
        target = at(y, x, zz)
        copy(own_gain, gains.at[core, z], gain_send, gain_recv, target).start()

        @pl.when(zz == 0)
        def _():
            copy(
                turned.at[0:TOK, :], taken.at[core, z, HALO:ROWS, :], take_send, take_recv, target
            ).start()

        @pl.when(zz > 0)
        def _():
            first = pl.multiple_of(jnp.maximum(zz * TOK - HALO, 0), 32)
            copy(
                turned.at[pl.ds(first, ROWS), :], taken.at[core, z], take_send, take_recv, target
            ).start()

    def gather_stream():
        gains[core, z] = own_gain[...]

        @pl.when(z == 0)
        def _():
            taken[core, z, HALO:ROWS, :] = turned[0:TOK, :]

        @pl.when(z > 0)
        def _():
            first = pl.multiple_of(jnp.maximum(z * TOK - HALO, 0), 32)
            taken[core, z] = turned[pl.ds(first, ROWS), :]

        drain(gains.at[0, 0:7], gain_recv)

        @pl.when(z == 0)
        def _():
            drain(taken.at[0, 0:7, HALO:ROWS, :], take_recv)

        @pl.when(z > 0)
        def _():
            drain(taken.at[0, 0:7], take_recv)

        to_next = copy(
            taken.at[core, :, TOK:ROWS, :],
            taken.at[core, :, 0:HALO, :],
            edge_send.at[0],
            edge_recv.at[0],
            (sp + 1, core),
        )
        docs_next = copy(docs, edge_docs, edge_send.at[1], edge_recv.at[1], (sp + 1, core))

        @pl.when(has_next)
        def _():
            to_next.start()
            docs_next.start()
            to_next.wait_send()
            docs_next.wait_send()

        @pl.when(has_edge)
        def _():
            to_next.wait_recv()
            docs_next.wait_recv()

        @pl.when(jnp.logical_and(z == 0, sp == 0))
        def _():
            taken[core, :, 0:HALO, :] = jnp.zeros((NZ, HALO, LANES), jnp.bfloat16)
            edge_docs[...] = jnp.full(edge_docs.shape, -1, jnp.int32)

        mine = taken.at[core]
        copy(mine, mine, pair_send.at[0], pair_recv.at[0], sibling).start()
        mine = gains.at[core]
        copy(mine, mine, pair_send.at[1], pair_recv.at[1], sibling).start()

    def windows():
        own = docs[pl.ds(z, 1), :].astype(jnp.float32)
        inside = docs[pl.ds(turn(z, -1, NZ), 1), :].astype(jnp.float32)

        def stood(row):
            return jnp.broadcast_to(row, (LANES, LANES)).T

        masks[HALO:ROWS, :] = stood(own)

        @pl.when(z > 0)
        def _():
            masks[0:HALO, :] = stood(inside)[LANES - HALO :, :]

        @pl.when(z == 0)
        def _():
            masks[0:HALO, :] = stood(edge_docs[NZ - 1 : NZ, :].astype(jnp.float32))[LANES - HALO :, :]

        column = masks[...]
        members = jnp.ones((ROWS, LANES), jnp.float32)
        for g in range(4):
            same = column == pltpu.roll(column, 2**g, 0)
            members = members + jnp.where(same, pltpu.roll(members, 2**g, 0), 0.0)
            counts[g] = members

    def same_doc(g):
        column = masks[...]
        return column == pltpu.roll(column, 2**g, 0)

    def block_of(k):
        return k % 2, k // 2

    def stream_in():
        pltpu.make_async_copy(taken.at[0], taken.at[0], pair_recv.at[0]).wait()
        pltpu.make_async_copy(gains.at[0], gains.at[0], pair_recv.at[1]).wait()
        for k in range(16):
            residual[block_of(k)] = taken[block_of(k)].astype(jnp.float32)

    def pooled_of(layer):
        squares = jnp.zeros((ROWS, LANES), jnp.float32)
        for k in range(16):
            r = residual[block_of(k)]
            squares = squares + r * r
        mean = jnp.sum(squares, axis=1, keepdims=True) * (1.0 / D)
        scale = lax.rsqrt(mean + 1e-06)
        total = jnp.zeros((ROWS, PW // 2), jnp.float32)
        for j in range(8):
            pieces, sides = [], []
            for k in (2 * j, 2 * j + 1):
                g = gains[k % 2, k // 2, layer : layer + 1, :]
                pieces.append((residual[block_of(k)] * scale * g).astype(jnp.bfloat16))
                sides.append(weights[2 * layer, k // NX, k % NX].reshape(PW // 2, LANES))
            total = total + lax.dot_general(
                jnp.concatenate(pieces, axis=1),
                jnp.concatenate(sides, axis=1),
                NT,
                preferred_element_type=jnp.float32,
            )
        pool_in = total.astype(jnp.bfloat16).astype(jnp.float32)
        groups = []
        for g in range(4):
            values = pool_in[:, g * LANES : (g + 1) * LANES]
            window = values
            for h in range(g + 1):
                window = window + jnp.where(same_doc(h), pltpu.roll(window, 2**h, 0), 0.0)
            groups.append((window / counts[g] - values).astype(jnp.bfloat16))
        return jnp.concatenate(groups, axis=1)

    def project_out(pooled):
        for j in range(8):
            side = [weights[1, k // NX, k % NX].reshape(PW // 2, LANES) for k in (2 * j, 2 * j + 1)]
            part = lax.dot_general(
                pooled, jnp.concatenate(side, axis=1), NN, preferred_element_type=jnp.float32
            )
            for h in range(2):
                piece = part[:, h * LANES : (h + 1) * LANES]
                residual[h, j] = residual[h, j] + piece
                sums_out[j, h] = piece.astype(jnp.bfloat16)
            if j % 2 == 1:
                pair = pl.ds(j - 1, 2)
                copy(
                    sums_out.at[pair], sums_in.at[pair], sums_send.at[j // 2], sums_recv.at[j // 2], sibling
                ).start()

    def add_sums():
        for q in range(4):
            pair = pl.ds(2 * q, 2)
            pltpu.make_async_copy(sums_in.at[pair], sums_in.at[pair], sums_recv.at[q]).wait()
            for j in (2 * q, 2 * q + 1):
                for h in range(2):
                    residual[h, j] = residual[h, j] + sums_in[j, h].astype(jnp.float32)

    order = (4, 3, 5, 2, 6, 1, 7, 0)

    def project_last(pooled):
        tail = pooled[HALO:, :]
        for i, d in enumerate(order):
            j = turn(z, d, NZ)
            yy, xx = j // 2, 2 * (j % 2)
            side = [weights[3, yy, xx + h].reshape(PW // 2, LANES) for h in range(2)]
            part = lax.dot_general(
                tail, jnp.concatenate(side, axis=1), NN, preferred_element_type=jnp.float32
            )
            low, high = part[:, :LANES], part[:, LANES:]
            last_out[i] = jnp.where(core == 0, high, low).astype(jnp.bfloat16)
            copy(last_out.at[i], last_in.at[i], last_send.at[i], last_recv.at[i], sibling).start()
            residual[core, j, HALO:ROWS, :] = residual[core, j, HALO:ROWS, :] + jnp.where(core == 0, low, high)
        lanes = pl.ds(pl.multiple_of(z * TOK, TOK), TOK)
        for i, d in enumerate(order):
            j = turn(z, d, NZ)
            pltpu.make_async_copy(last_in.at[i], last_in.at[i], last_recv.at[i]).wait()
            done = residual[core, j, HALO:ROWS, :] + last_in[i].astype(jnp.float32)
            if d == 0:
                out[:, lanes] = done.T.astype(jnp.bfloat16)
            else:
                mixed[i] = done.T.astype(jnp.bfloat16)
                copy(mixed.at[i], out.at[:, lanes], mixed_send, mixed_recv, at(y, x, j)).start()

    drain(weights.at[0, 0, 0:2, 0:6], plane_recv)
    send_z(0, 0)
    send_line(0, 0)
    pooled = None
    for w in range(WAVES):
        for step in range(1, 5):
            wait_z(w, step)
            if step < 4:
                send_z(w, step)
            if step == 2 and w + 1 < WAVES:
                send_z(w + 1, 0)
            send_line(w, step)
            pass_on(w, step - 1)
            if w == 0:
                for d in ((1, 7), (2, 6), (3, 5), (4,))[step - 1]:
                    send_taken(d)
            if w == 1 and step == 1:
                gather_stream()
                windows()
            if w > 0 and step == 2:
                wait_far(w - 1)
                if w == 1:
                    stream_in()
                    pooled = pooled_of(0)
                if w == 2:
                    project_out(pooled)
                if w == 3:
                    add_sums()
                    pooled = pooled_of(1)
            if step == 4 and w + 1 < WAVES:
                send_line(w + 1, 0)
        pass_on(w, 4)
    wait_far(3)
    project_last(pooled)

    drain(out.at[:, 0 : 7 * TOK], mixed_recv)
    drain(mixed.at[0:7], mixed_send)
    drain(weights.at[0, 0, 0:2, 0:6], plane_send)
    for w in range(WAVES):
        drain(weights.at[w, 0, :, 0:7], z_send.at[w])
        drain(weights.at[w, 0:3], line_send.at[w])
    drain(gains.at[0, 0:7], gain_send)

    @pl.when(z == 0)
    def _():
        drain(taken.at[0, 0:7], take_send)

    @pl.when(z > 0)
    def _():
        drain(taken.at[0, :, 0 : ROWS - 24, :], take_send)

    pltpu.make_async_copy(taken.at[0], taken.at[0], pair_send.at[0]).wait()
    pltpu.make_async_copy(gains.at[0], gains.at[0], pair_send.at[1]).wait()
    for q in range(4):
        pair = pl.ds(2 * q, 2)
        pltpu.make_async_copy(sums_out.at[pair], sums_out.at[pair], sums_send.at[q]).wait()
    for i in range(8):
        pltpu.make_async_copy(last_out.at[i], last_out.at[i], last_send.at[i]).wait()


def per_device(stream, norm_gain, in_weight, out_weight, docs):
    vmem = pl.BlockSpec(memory_space=pltpu.VMEM)
    dma = pltpu.SemaphoreType.DMA
    bf16, f32 = jnp.bfloat16, jnp.float32
    return pl.pallas_call(
        kernel,
        out_shape=jax.ShapeDtypeStruct(stream.shape, bf16),
        in_specs=[vmem] * 5,
        out_specs=vmem,
        scratch_shapes=[
            pltpu.VMEM((WAVES, NY, NX, NZ, 64, LANES), bf16),
            pltpu.VMEM((NZ * TOK, LANES), bf16),
            pltpu.VMEM((2, NZ, ROWS, LANES), bf16),
            pltpu.VMEM((2, NZ, 8, LANES), f32),
            pltpu.VMEM((8, LANES), f32),
            pltpu.VMEM((NZ, LANES), jnp.int32),
            pltpu.VMEM((2, NZ, ROWS, LANES), f32),
            pltpu.VMEM((NZ, 2, ROWS, LANES), bf16),
            pltpu.VMEM((NZ, 2, ROWS, LANES), bf16),
            pltpu.VMEM((NZ, TOK, LANES), bf16),
            pltpu.VMEM((NZ, TOK, LANES), bf16),
            pltpu.VMEM((NZ, TOK, LANES), bf16),
            pltpu.VMEM((ROWS, LANES), f32),
            pltpu.VMEM((4, ROWS, LANES), f32),
            dma,
            dma,
            dma((WAVES,)),
            dma((WAVES, 4)),
            dma((WAVES,)),
            dma((WAVES, 5)),
            dma((WAVES,)),
            dma,
            dma,
            dma,
            dma,
            dma((2,)),
            dma((2,)),
            dma((2,)),
            dma((2,)),
            dma((4,)),
            dma((4,)),
            dma((8,)),
            dma((8,)),
            dma,
            dma,
        ],
        compiler_params=pltpu.CompilerParams(collective_id=0, has_side_effects=True),
    )(stream, norm_gain, in_weight, out_weight, docs.reshape(NZ, LANES))


def solution(mesh):
    return jax.shard_map(
        per_device,
        mesh=mesh,
        in_specs=(P("tp", "sp"), P(None, "tp"), P(None, "sp", "tp"), P(None, "tp", "sp"), P("sp")),
        out_specs=P("tp", "sp"),
        check_vma=False,
    )
```

time: 236 us -> 101 us (0.43)
  Pallas kernels: 0 us -> 98 us
  blocking collectives: 96.8 us -> 0 us
  waiting for transfers between devices: 83.9 us -> 0 us
  starting transfers between devices: 19 us -> 0 us
  between operations: 13.3 us -> 0.01 us
  matrix products: 10.9 us -> 0 us
  other arithmetic: 8.37 us -> 0 us
    pallas_call x0 -> x1, Pallas kernels: none -> 98 us  [per_device(): pl.pallas_call(kernel, out_shape=jax.ShapeDtypeStruct(stream.shape, bf16)...]
    all_gather x4 -> x0, waiting for transfers between devices: 68.4 us -> none  [the longest x2 47.1 us: whole_of(): array = lax.all_gather(array, axis, axis=dim, tiled=True)]
    all_gather x4 -> x0, blocking collectives: 52.3 us -> none  [the longest x2 48 us: rows_first(): result = lax.all_gather(both, axis, axis=0, tiled=True)]
    all_to_all x3 -> x0, blocking collectives: 44.5 us -> none  [the longest x2 32.4 us: per_device(): lax.all_to_all(out_rows, TP, split_axis=1, concat_axis=0, tiled=True)]
    dot_general x4 -> x0, matrix products: 10.9 us -> none  [the longest x2 6.06 us: per_device(): lax.dot_general(in_block, lax.all_gather(normed, TP, axis=0, tiled=True),...]
    ppermute x3 -> x0, starting transfers between devices: 10.3 us -> none  [passed_along(): return lax.ppermute(block, axis, route)]
    all_to_all x1 -> x0, starting transfers between devices: 8.57 us -> none  [sent_to_all(): return lax.all_to_all(copies, axis, split_axis=0, concat_axis=0, tiled=True)]
    ppermute x3 -> x0, waiting for transfers between devices: 8.48 us -> none  [passed_along(): return lax.ppermute(block, axis, route)]
  transfers between devices with their start and end apart: 8 -> 0, of which waited for: 7 -> 0; matrix products, arithmetic and copies ran while one was open for 2% -> 0% of each run, Pallas kernels for 0% -> 0%
where the time goes in v1:
time: 101 us
  Pallas kernels  98 us (97%)
  local copies, waits for them, and re-layouts  3.16 us (3%)
    pallas_call x1, Pallas kernels, per_device(): pl.pallas_call(kernel, out_shape=jax.ShapeDtypeStruct(stream.shape, bf16)...  98 us
    unnamed x2, local copies, waits for them, and re-layouts  3.16 us

profile of v1, /device:TPU:8, one launch (start us, length us, event | category | flops | bytes accessed | tf_op | source)
XLA Modules:
  0.0 101.1 jit_solution(16768460204088880901)
XLA Ops:
  0.0 1.5 %copy.6.in_w = bf16[2,128,64]{2,1,0:T(8,128)(2,1)} copy(bf16[2,128,64]{1,2,0:T(8,128)(2,1)} %param.7) | data formatting | bytes 65536 | tf_op args[2]
  1.5 98.0 %shard_map.55 = bf16[128,1024]{1,0:T(8,128)(2,1)} custom-call(bf16[128,1024]{1,0:T(8,128)(2,1)} %stream.1, f32[2,128]{1,0:T(2,128)} %gain.1, bf16[2,128,64]{2,1,0:T(8,128)(2,1)} %copy.6.in_w, bf16[2,64,128]{2,1,0:T(8,128)(2,1)} %out_w.1, s32[8,128]{1,0:T(8,128)} %bitcast.1), custom_call_target="tpu_custom_call" | custom-call | tf_op jit(solution)/shard_map/pallas_call | solution.py:422
  99.5 1.7 %copy.8 = bf16[128,1024]{1,0:T(8,128)(2,1)} copy(bf16[128,1024]{1,0:T(8,128)(2,1)} %shard_map.55) | data formatting | bytes 524288

commit v2 on v1

--- a/solution.py
+++ b/solution.py
@@ -108,7 +108,7 @@
         )
 
     for layer in range(LAYERS):
-        weights[2 * layer, y, x, z] = in_w[layer].astype(jnp.float32).T.astype(jnp.bfloat16)
+        weights[2 * layer, y, x, z] = in_w[layer]
         weights[2 * layer + 1, y, x, z] = out_w[layer]
     for j in range(NZ):
         block = stream[:, j * TOK : (j + 1) * TOK].astype(jnp.float32)
@@ -119,12 +119,13 @@
     extra = jnp.logical_or(has_next, has_edge).astype(jnp.int32)
     pl.semaphore_wait(barrier, len(peers) + extra)
 
-    for d in range(1, NY):
-        part = weights.at[:, y, x, z, 0:HALF, :]
-        copy(part, part, plane_send, plane_recv, at(turn(y, d, NY), x, z)).start()
-    for d in range(1, NX):
-        part = weights.at[:, y, x, z, HALF : 2 * HALF, :]
-        copy(part, part, plane_send, plane_recv, at(y, turn(x, d, NX), z)).start()
+    for group, waves in enumerate((slice(0, 1), slice(1, WAVES))):
+        for d in range(1, NY):
+            part = weights.at[waves, y, x, z, 0:HALF, :]
+            copy(part, part, plane_send, plane_recv.at[group], at(turn(y, d, NY), x, z)).start()
+        for d in range(1, NX):
+            part = weights.at[waves, y, x, z, HALF : 2 * HALF, :]
+            copy(part, part, plane_send, plane_recv.at[group], at(y, turn(x, d, NX), z)).start()
 
     def slab_a(w, xx, zz):
         return weights.at[w, :, xx, zz, 0:HALF, :]
@@ -355,38 +356,47 @@
                 mixed[i] = done.T.astype(jnp.bfloat16)
                 copy(mixed.at[i], out.at[:, lanes], mixed_send, mixed_recv, at(y, x, j)).start()
 
-    drain(weights.at[0, 0, 0:2, 0:6], plane_recv)
+    drain(weights.at[0, 0, 0, 0:3], plane_recv.at[0])
     send_z(0, 0)
     send_line(0, 0)
-    pooled = None
-    for w in range(WAVES):
-        for step in range(1, 5):
-            wait_z(w, step)
-            if step < 4:
-                send_z(w, step)
-            if step == 2 and w + 1 < WAVES:
-                send_z(w + 1, 0)
-            send_line(w, step)
-            pass_on(w, step - 1)
-            if w == 0:
-                for d in ((1, 7), (2, 6), (3, 5), (4,))[step - 1]:
-                    send_taken(d)
-            if w == 1 and step == 1:
-                gather_stream()
-                windows()
-            if w > 0 and step == 2:
-                wait_far(w - 1)
-                if w == 1:
-                    stream_in()
-                    pooled = pooled_of(0)
-                if w == 2:
-                    project_out(pooled)
-                if w == 3:
-                    add_sums()
-                    pooled = pooled_of(1)
-            if step == 4 and w + 1 < WAVES:
-                send_line(w + 1, 0)
-        pass_on(w, 4)
+    drain(weights.at[0, 0, 0:3, 0:3], plane_recv.at[1])
+    send_z(1, 0)
+    send_line(1, 0)
+
+    def pass_on_tick(tick):
+        for w in range(WAVES):
+            if 0 <= tick - w <= 4:
+                pass_on(w, tick - w)
+
+    for tick in range(1, WAVES + 4):
+        for w in range(WAVES):
+            step = tick - w
+            if 1 <= step <= 4:
+                wait_z(w, step)
+                if step < 4:
+                    send_z(w, step)
+                send_line(w, step)
+        if tick + 1 < WAVES:
+            send_z(tick + 1, 0)
+            send_line(tick + 1, 0)
+        if tick <= 4:
+            for d in ((1, 7), (2, 6), (3, 5), (4,))[tick - 1]:
+                send_taken(d)
+        if tick >= 2:
+            pass_on_tick(tick - 2)
+        if tick == 6:
+            gather_stream()
+            windows()
+    wait_far(0)
+    stream_in()
+    pooled = pooled_of(0)
+    pass_on_tick(6)
+    wait_far(1)
+    project_out(pooled)
+    pass_on_tick(7)
+    wait_far(2)
+    add_sums()
+    pooled = pooled_of(1)
     wait_far(3)
     project_last(pooled)
 
@@ -440,7 +450,7 @@
             pltpu.VMEM((ROWS, LANES), f32),
             pltpu.VMEM((4, ROWS, LANES), f32),
             dma,
-            dma,
+            dma((2,)),
             dma((WAVES,)),
             dma((WAVES, 4)),
             dma((WAVES,)),
@@ -462,7 +472,7 @@
             dma,
         ],
         compiler_params=pltpu.CompilerParams(collective_id=0, has_side_effects=True),
-    )(stream, norm_gain, in_weight, out_weight, docs.reshape(NZ, LANES))
+    )(stream, norm_gain, jnp.swapaxes(in_weight, 1, 2), out_weight, docs.reshape(NZ, LANES))
 
 
 def solution(mesh):

time: 101 us -> 71.2 us (0.70); the launches traced: 101 us -> 69.9 us
  Pallas kernels: 98 us -> 68.2 us
  local copies, waits for them, and re-layouts: 3.16 us -> 1.67 us
    pallas_call x1, Pallas kernels: 98 us -> 68.2 us  [per_device(): pl.pallas_call(kernel, out_shape=jax.ShapeDtypeStruct(stream.shape, bf16)...]
    unnamed x2 -> x1, local copies, waits for them, and re-layouts: 3.16 us -> 1.67 us
where the time goes in v2:
time: 71.2 us; the launch traced here: 69.9 us
  Pallas kernels  68.2 us (96%)
  local copies, waits for them, and re-layouts  1.67 us (2%)
    pallas_call x1, Pallas kernels, per_device(): pl.pallas_call(kernel, out_shape=jax.ShapeDtypeStruct(stream.shape, bf16)...  68.2 us
    unnamed x1, local copies, waits for them, and re-layouts  1.67 us

profile of v2, /device:TPU:8, one launch (start us, length us, event | category | flops | bytes accessed | tf_op | source)
XLA Modules:
  0.0 69.9 jit_solution(2897071729348567850)
XLA Ops:
  0.0 68.2 %shard_map.55 = bf16[128,1024]{1,0:T(8,128)(2,1)} custom-call(bf16[128,1024]{1,0:T(8,128)(2,1)} %stream.1, f32[2,128]{1,0:T(2,128)} %gain.1, bf16[2,64,128]{2,1,0:T(8,128)(2,1)} %bitcast.2, bf16[2,64,128]{2,1,0:T(8,128)(2,1)} %out_w.1, s32[8,128]{1,0:T(8,128)} %bitcast.3), custom_call_target="tpu_custom_call" | custom-call | tf_op jit(solution)/shard_map/pallas_call | solution.py:432
  68.2 1.7 %copy.7 = bf16[128,1024]{1,0:T(8,128)(2,1)} copy(bf16[128,1024]{1,0:T(8,128)(2,1)} %shard_map.55) | data formatting | bytes 524288

commit v3 on v2

--- a/solution.py
+++ b/solution.py
@@ -24,12 +24,15 @@
 
 
 def kernel(
+    stream_hbm,
+    gain_hbm,
+    in_w,
+    out_w,
+    docs_hbm,
+    out,
     stream,
     gain,
-    in_w,
-    out_w,
     docs,
-    out,
     weights,
     turned,
     taken,
@@ -37,6 +40,7 @@
     own_gain,
     edge_docs,
     residual,
+    normed,
     sums_out,
     sums_in,
     last_out,
@@ -44,6 +48,7 @@
     mixed,
     masks,
     counts,
+    load,
     plane_send,
     plane_recv,
     z_send,
@@ -107,19 +112,33 @@
             barrier, inc=1, device_id=(sp - 1, (NZ - 1) * 2 + core), device_id_type=MESH
         )
 
+    loads = []
     for layer in range(LAYERS):
-        weights[2 * layer, y, x, z] = in_w[layer]
-        weights[2 * layer + 1, y, x, z] = out_w[layer]
-    for j in range(NZ):
-        block = stream[:, j * TOK : (j + 1) * TOK].astype(jnp.float32)
-        turned[j * TOK : (j + 1) * TOK, :] = block.T.astype(jnp.bfloat16)
-    own_gain[...] = jnp.zeros_like(own_gain)
-    own_gain[0:LAYERS, :] = gain[...]
+        for i, source in enumerate((in_w, out_w)):
+            w = 2 * layer + i
+            loads.append(pltpu.make_async_copy(source.at[layer], weights.at[w, y, x, z], load.at[w]))
+    loads.append(pltpu.make_async_copy(stream_hbm, stream, load.at[4]))
+    loads.append(pltpu.make_async_copy(gain_hbm, gain, load.at[5]))
+    loads.append(pltpu.make_async_copy(docs_hbm, docs, load.at[6]))
+    for one in loads:
+        one.start()
+    for one in loads[:4]:
+        one.wait()
+
+    def turn_stream():
+        for one in loads[4:]:
+            one.wait()
+        for j in range(NZ):
+            block = stream[:, j * TOK : (j + 1) * TOK].astype(jnp.float32)
+            turned[j * TOK : (j + 1) * TOK, :] = block.T.astype(jnp.bfloat16)
+        own_gain[...] = jnp.zeros_like(own_gain)
+        own_gain[0:LAYERS, :] = gain[...]
 
     extra = jnp.logical_or(has_next, has_edge).astype(jnp.int32)
     pl.semaphore_wait(barrier, len(peers) + extra)
 
-    for group, waves in enumerate((slice(0, 1), slice(1, WAVES))):
+    def send_plane(group):
+        waves = (slice(0, 1), slice(1, WAVES))[group]
         for d in range(1, NY):
             part = weights.at[waves, y, x, z, 0:HALF, :]
             copy(part, part, plane_send, plane_recv.at[group], at(turn(y, d, NY), x, z)).start()
@@ -133,28 +152,49 @@
     def slab_b(w, yy, zz):
         return weights.at[w, yy, :, zz, HALF : 2 * HALF, :]
 
-    def send_z(w, step):
+    def ring_a(w, step):
         up, down = at(y, x, turn(z, 1, NZ)), at(y, x, turn(z, -1, NZ))
-        before, after = turn(z, -step, NZ), turn(z, step, NZ)
-        send, recv = z_send.at[w], z_recv.at[w, step]
-        a, b = slab_a(w, x, before), slab_b(w, y, after)
-        copy(a, a, send, recv, up).start()
-        copy(b, b, send, recv, down).start()
+        slab = slab_a(w, x, turn(z, -step, NZ))
+        copy(slab, slab, z_send.at[w], z_recv.at[0, w, step], up).start()
         if step < 3:
-            a, b = slab_a(w, x, after), slab_b(w, y, before)
-            copy(a, a, send, recv, down).start()
-            copy(b, b, send, recv, up).start()
-
-    def wait_z(w, step):
-        drain(weights.at[w, 0, 0, 0 : (8 if step < 4 else 4)], z_recv.at[w, step - 1])
-
-    def send_line(w, step):
+            slab = slab_a(w, x, turn(z, step, NZ))
+            copy(slab, slab, z_send.at[w], z_recv.at[0, w, step], down).start()
+
+    def ring_b(w, step):
+        up, down = at(y, x, turn(z, 1, NZ)), at(y, x, turn(z, -1, NZ))
+        slab = slab_b(w, y, turn(z, step, NZ))
+        copy(slab, slab, z_send.at[w], z_recv.at[1, w, step], down).start()
+        if step < 3:
+            slab = slab_b(w, y, turn(z, -step, NZ))
+            copy(slab, slab, z_send.at[w], z_recv.at[1, w, step], up).start()
+
+    def line_a(w, step):
         for offset in STEP_OFFSETS[step]:
-            zz = turn(z, offset, NZ)
-            a, b = slab_a(w, x, zz), slab_b(w, y, zz)
+            slab = slab_a(w, x, turn(z, offset, NZ))
             for side in (1, -1):
-                copy(a, a, line_send.at[w], line_recv.at[w, step], at(y, turn(x, side, NX), z)).start()
-                copy(b, b, line_send.at[w], line_recv.at[w, step], at(turn(y, side, NY), x, z)).start()
+                to = at(y, turn(x, side, NX), z)
+                copy(slab, slab, line_send.at[w], line_recv.at[w, step], to).start()
+
+    def line_b(w, step):
+        for offset in STEP_OFFSETS[step]:
+            slab = slab_b(w, y, turn(z, offset, NZ))
+            for side in (1, -1):
+                to = at(turn(y, side, NY), x, z)
+                copy(slab, slab, line_send.at[w], line_recv.at[w, step], to).start()
+
+    def first_step(w):
+        ring_a(w, 0)
+        ring_b(w, 0)
+
+    def along_lines(w, step):
+        line_a(w, step)
+        line_b(w, step)
+
+    def ring_step(w, step):
+        for part, ring in ((0, ring_a), (1, ring_b)):
+            drain(weights.at[w, 0, 0, 0 : (4 if step < 4 else 2)], z_recv.at[part, w, step - 1])
+            if step < 4:
+                ring(w, step)
 
     def pass_on(w, step):
         drain(weights.at[w, 0, 0 : len(STEP_OFFSETS[step])], line_recv.at[w, step])
@@ -276,25 +316,24 @@
         for k in range(16):
             residual[block_of(k)] = taken[block_of(k)].astype(jnp.float32)
 
-    def pooled_of(layer):
+    def normalize(layer):
         squares = jnp.zeros((ROWS, LANES), jnp.float32)
         for k in range(16):
             r = residual[block_of(k)]
             squares = squares + r * r
         mean = jnp.sum(squares, axis=1, keepdims=True) * (1.0 / D)
         scale = lax.rsqrt(mean + 1e-06)
+        for k in range(16):
+            g = gains[k % 2, k // 2, layer : layer + 1, :]
+            side = slice((k % 2) * LANES, (k % 2 + 1) * LANES)
+            normed[k // 2, :, side] = (residual[block_of(k)] * scale * g).astype(jnp.bfloat16)
+
+    def pooled_of(layer):
         total = jnp.zeros((ROWS, PW // 2), jnp.float32)
         for j in range(8):
-            pieces, sides = [], []
-            for k in (2 * j, 2 * j + 1):
-                g = gains[k % 2, k // 2, layer : layer + 1, :]
-                pieces.append((residual[block_of(k)] * scale * g).astype(jnp.bfloat16))
-                sides.append(weights[2 * layer, k // NX, k % NX].reshape(PW // 2, LANES))
+            sides = [weights[2 * layer, k // NX, k % NX].reshape(PW // 2, LANES) for k in (2 * j, 2 * j + 1)]
             total = total + lax.dot_general(
-                jnp.concatenate(pieces, axis=1),
-                jnp.concatenate(sides, axis=1),
-                NT,
-                preferred_element_type=jnp.float32,
+                normed[j], jnp.concatenate(sides, axis=1), NT, preferred_element_type=jnp.float32
             )
         pool_in = total.astype(jnp.bfloat16).astype(jnp.float32)
         groups = []
@@ -330,75 +369,162 @@
                 for h in range(2):
                     residual[h, j] = residual[h, j] + sums_in[j, h].astype(jnp.float32)
 
-    order = (4, 3, 5, 2, 6, 1, 7, 0)
-
-    def project_last(pooled):
-        tail = pooled[HALO:, :]
-        for i, d in enumerate(order):
-            j = turn(z, d, NZ)
-            yy, xx = j // 2, 2 * (j % 2)
-            side = [weights[3, yy, xx + h].reshape(PW // 2, LANES) for h in range(2)]
-            part = lax.dot_general(
-                tail, jnp.concatenate(side, axis=1), NN, preferred_element_type=jnp.float32
-            )
-            low, high = part[:, :LANES], part[:, LANES:]
-            last_out[i] = jnp.where(core == 0, high, low).astype(jnp.bfloat16)
-            copy(last_out.at[i], last_in.at[i], last_send.at[i], last_recv.at[i], sibling).start()
-            residual[core, j, HALO:ROWS, :] = residual[core, j, HALO:ROWS, :] + jnp.where(core == 0, low, high)
+    mine = (core + x) % 2
+
+    def last_pair(i):
+        if i < 3:
+            turned_by = (i + z) % 3
+            dy, dx = turned_by + turned_by // 2, 0
+        else:
+            turned_by = (i + z) % 5
+            beyond = turned_by // 3
+            dy = (1 - beyond) * (turned_by + turned_by // 2) + 2 * beyond
+            dx = 2 - 2 * beyond * (4 - turned_by)
+        yy = (y + dy) % NY
+        return yy, (x + dx + mine) % NX, (x + dx + 1 - mine) % NX
+
+    def last_dot(i, tail):
+        yy, x_own, x_other = last_pair(i)
+        side = [weights[3, yy, xx].reshape(PW // 2, LANES) for xx in (x_own, x_other)]
+        part = lax.dot_general(tail, jnp.concatenate(side, axis=1), NN, preferred_element_type=jnp.float32)
+        last_out[i] = part[:, LANES:].astype(jnp.bfloat16)
+        copy(last_out.at[i], last_in.at[i], last_send.at[i], last_recv.at[i], sibling).start()
+        j = 2 * yy + x_own // 2
+        residual[core, j, HALO:ROWS, :] = residual[core, j, HALO:ROWS, :] + part[:, :LANES]
+
+    def last_turn(i):
+        yy, x_own, _ = last_pair(i)
+        j = 2 * yy + x_own // 2
+        pltpu.make_async_copy(last_in.at[i], last_in.at[i], last_recv.at[i]).wait()
+        done = residual[core, j, HALO:ROWS, :] + last_in[i].astype(jnp.float32)
+        mixed[i] = done.T.astype(jnp.bfloat16)
         lanes = pl.ds(pl.multiple_of(z * TOK, TOK), TOK)
-        for i, d in enumerate(order):
-            j = turn(z, d, NZ)
-            pltpu.make_async_copy(last_in.at[i], last_in.at[i], last_recv.at[i]).wait()
-            done = residual[core, j, HALO:ROWS, :] + last_in[i].astype(jnp.float32)
-            if d == 0:
-                out[:, lanes] = done.T.astype(jnp.bfloat16)
-            else:
-                mixed[i] = done.T.astype(jnp.bfloat16)
-                copy(mixed.at[i], out.at[:, lanes], mixed_send, mixed_recv, at(y, x, j)).start()
-
-    drain(weights.at[0, 0, 0, 0:3], plane_recv.at[0])
-    send_z(0, 0)
-    send_line(0, 0)
-    drain(weights.at[0, 0, 0:3, 0:3], plane_recv.at[1])
-    send_z(1, 0)
-    send_line(1, 0)
-
-    def pass_on_tick(tick):
-        for w in range(WAVES):
-            if 0 <= tick - w <= 4:
-                pass_on(w, tick - w)
-
-    for tick in range(1, WAVES + 4):
-        for w in range(WAVES):
-            step = tick - w
-            if 1 <= step <= 4:
-                wait_z(w, step)
-                if step < 4:
-                    send_z(w, step)
-                send_line(w, step)
-        if tick + 1 < WAVES:
-            send_z(tick + 1, 0)
-            send_line(tick + 1, 0)
-        if tick <= 4:
-            for d in ((1, 7), (2, 6), (3, 5), (4,))[tick - 1]:
-                send_taken(d)
-        if tick >= 2:
-            pass_on_tick(tick - 2)
-        if tick == 6:
-            gather_stream()
-            windows()
-    wait_far(0)
-    stream_in()
-    pooled = pooled_of(0)
-    pass_on_tick(6)
-    wait_far(1)
-    project_out(pooled)
-    pass_on_tick(7)
-    wait_far(2)
-    add_sums()
-    pooled = pooled_of(1)
-    wait_far(3)
-    project_last(pooled)
+
+        @pl.when(j == z)
+        def _():
+            out[:, lanes] = mixed[i]
+
+        @pl.when(j != z)
+        def _():
+            copy(mixed.at[i], out.at[:, lanes], mixed_send, mixed_recv, at(y, x, j)).start()
+
+    def first_arrived(group):
+        drain(weights.at[0, 0, 0, 0:3] if group == 0 else weights.at[0, 0, 0:3, 0:3], plane_recv.at[group])
+
+    def stream_ready():
+        stream_in()
+        normalize(0)
+
+    held = {}
+
+    def project_0():
+        wait_far(0)
+        held["pooled"] = pooled_of(0)
+
+    def project_1():
+        wait_far(1)
+        project_out(held["pooled"])
+
+    def settle():
+        add_sums()
+        normalize(1)
+
+    def project_2():
+        wait_far(2)
+        held["pooled"] = pooled_of(1)
+
+    def project_3():
+        tail = held["pooled"][HALO:, :]
+        for i in range(3):
+            last_dot(i, tail)
+        for i in range(3):
+            last_turn(i)
+        wait_far(3)
+        for i in range(3, 8):
+            last_dot(i, tail)
+        for i in range(3, 8):
+            last_turn(i)
+
+    send_plane(0)
+    send_plane(1)
+    turn_stream()
+    send_taken(1)
+    send_taken(7)
+    send_taken(2)
+    send_taken(6)
+    first_arrived(0)
+    first_step(0)
+    along_lines(0, 0)
+    first_arrived(1)
+    first_step(1)
+    first_step(2)
+    first_step(3)
+    along_lines(1, 0)
+    along_lines(2, 0)
+    along_lines(3, 0)
+    ring_step(0, 1)
+    along_lines(0, 1)
+    ring_step(1, 1)
+    along_lines(1, 1)
+    pass_on(0, 0)
+    ring_step(2, 1)
+    pass_on(1, 0)
+    ring_step(3, 1)
+    pass_on(2, 0)
+    pass_on(3, 0)
+    along_lines(2, 1)
+    ring_step(0, 2)
+    along_lines(0, 2)
+    pass_on(0, 1)
+    ring_step(1, 2)
+    along_lines(1, 2)
+    pass_on(1, 1)
+    ring_step(2, 2)
+    send_taken(3)
+    ring_step(3, 2)
+    send_taken(5)
+    ring_step(0, 3)
+    along_lines(0, 3)
+    pass_on(0, 2)
+    ring_step(1, 3)
+    along_lines(1, 3)
+    pass_on(1, 2)
+    ring_step(2, 3)
+    send_taken(4)
+    along_lines(3, 1)
+    pass_on(2, 1)
+    ring_step(3, 3)
+    along_lines(2, 2)
+    ring_step(0, 4)
+    along_lines(0, 4)
+    pass_on(0, 3)
+    ring_step(1, 4)
+    along_lines(1, 4)
+    pass_on(1, 3)
+    ring_step(2, 4)
+    along_lines(2, 3)
+    along_lines(2, 4)
+    pass_on(3, 1)
+    ring_step(3, 4)
+    along_lines(3, 2)
+    along_lines(3, 3)
+    along_lines(3, 4)
+    pass_on(0, 4)
+    pass_on(2, 2)
+    gather_stream()
+    windows()
+    pass_on(1, 4)
+    stream_ready()
+    project_0()
+    pass_on(2, 3)
+    pass_on(2, 4)
+    pass_on(3, 2)
+    project_1()
+    pass_on(3, 3)
+    pass_on(3, 4)
+    settle()
+    project_2()
+    project_3()
 
     drain(out.at[:, 0 : 7 * TOK], mixed_recv)
     drain(mixed.at[0:7], mixed_send)
@@ -431,10 +557,13 @@
     bf16, f32 = jnp.bfloat16, jnp.float32
     return pl.pallas_call(
         kernel,
-        out_shape=jax.ShapeDtypeStruct(stream.shape, bf16),
-        in_specs=[vmem] * 5,
+        out_shape=pltpu.VMEM(stream.shape, bf16),
+        in_specs=[pl.BlockSpec(memory_space=pl.ANY)] * 5,
         out_specs=vmem,
         scratch_shapes=[
+            pltpu.VMEM((LANES, NZ * TOK), bf16),
+            pltpu.VMEM((LAYERS, LANES), f32),
+            pltpu.VMEM((NZ, LANES), jnp.int32),
             pltpu.VMEM((WAVES, NY, NX, NZ, 64, LANES), bf16),
             pltpu.VMEM((NZ * TOK, LANES), bf16),
             pltpu.VMEM((2, NZ, ROWS, LANES), bf16),
@@ -442,6 +571,7 @@
             pltpu.VMEM((8, LANES), f32),
             pltpu.VMEM((NZ, LANES), jnp.int32),
             pltpu.VMEM((2, NZ, ROWS, LANES), f32),
+            pltpu.VMEM((NZ, ROWS, 2 * LANES), bf16),
             pltpu.VMEM((NZ, 2, ROWS, LANES), bf16),
             pltpu.VMEM((NZ, 2, ROWS, LANES), bf16),
             pltpu.VMEM((NZ, TOK, LANES), bf16),
@@ -449,10 +579,11 @@
             pltpu.VMEM((NZ, TOK, LANES), bf16),
             pltpu.VMEM((ROWS, LANES), f32),
             pltpu.VMEM((4, ROWS, LANES), f32),
+            dma((7,)),
             dma,
             dma((2,)),
             dma((WAVES,)),
-            dma((WAVES, 4)),
+            dma((2, WAVES, 4)),
             dma((WAVES,)),
             dma((WAVES, 5)),
             dma((WAVES,)),

time: 71.2 us -> 64.1 us (0.900)
  Pallas kernels: 68.2 us -> 62.5 us
  local copies, waits for them, and re-layouts: 1.67 us -> 0.71 us
    pallas_call x1, Pallas kernels: 68.2 us -> 62.5 us  [per_device(): pl.pallas_call(kernel, out_shape=pltpu.VMEM(stream.shape, bf16), in_specs...]
    unnamed x1, local copies, waits for them, and re-layouts: 1.67 us -> 0.71 us
where the time goes in v3:
time: 64.1 us; the launch traced here: 63.2 us
  Pallas kernels  62.5 us (98%)
  local copies, waits for them, and re-layouts  0.71 us (1%)
    pallas_call x1, Pallas kernels, per_device(): pl.pallas_call(kernel, out_shape=pltpu.VMEM(stream.shape, bf16), in_specs...  62.5 us

profile of v3, /device:TPU:8, one launch (start us, length us, event | category | flops | bytes accessed | tf_op | source)
XLA Modules:
  0.0 63.2 jit_solution(2892059372240728870)
XLA Ops:
  0.0 62.5 %shard_map.55 = bf16[128,1024]{1,0:T(8,128)(2,1)S(1)} custom-call(bf16[128,1024]{1,0:T(8,128)(2,1)} %stream_hbm.1, f32[2,128]{1,0:T(2,128)} %gain_hbm.1, bf16[2,64,128]{2,1,0:T(8,128)(2,1)} %bitcast.2, bf16[2,64,128]{2,1,0:T(8,128)(2,1)} %out_w.1, s32[8,128]{1,0:T(8,128)} %bitcast.3), custom_call_target="tpu_custom_call" | custom-call | tf_op jit(solution)/shard_map/pallas_call | solution.py:558
  62.5 0.7 %copy.7 = bf16[128,1024]{1,0:T(8,128)(2,1)} copy(bf16[128,1024]{1,0:T(8,128)(2,1)S(1)} %shard_map.55) | data formatting | bytes 524288

commit v4 on v3

--- a/solution.py
+++ b/solution.py
@@ -466,62 +466,62 @@
     along_lines(0, 1)
     ring_step(1, 1)
     along_lines(1, 1)
-    pass_on(0, 0)
     ring_step(2, 1)
-    pass_on(1, 0)
+    along_lines(2, 1)
     ring_step(3, 1)
-    pass_on(2, 0)
-    pass_on(3, 0)
-    along_lines(2, 1)
+    along_lines(3, 1)
     ring_step(0, 2)
     along_lines(0, 2)
-    pass_on(0, 1)
     ring_step(1, 2)
     along_lines(1, 2)
-    pass_on(1, 1)
     ring_step(2, 2)
-    send_taken(3)
+    along_lines(2, 2)
+    pass_on(0, 0)
     ring_step(3, 2)
-    send_taken(5)
+    along_lines(3, 2)
+    pass_on(1, 0)
     ring_step(0, 3)
     along_lines(0, 3)
-    pass_on(0, 2)
+    pass_on(2, 0)
     ring_step(1, 3)
     along_lines(1, 3)
-    pass_on(1, 2)
+    send_taken(3)
+    pass_on(3, 0)
     ring_step(2, 3)
+    along_lines(2, 3)
+    send_taken(5)
+    pass_on(0, 1)
+    ring_step(3, 3)
+    along_lines(3, 3)
     send_taken(4)
-    along_lines(3, 1)
-    pass_on(2, 1)
-    ring_step(3, 3)
-    along_lines(2, 2)
+    pass_on(1, 1)
     ring_step(0, 4)
     along_lines(0, 4)
-    pass_on(0, 3)
+    pass_on(2, 1)
     ring_step(1, 4)
     along_lines(1, 4)
+    pass_on(3, 1)
+    ring_step(2, 4)
+    along_lines(2, 4)
+    pass_on(0, 2)
+    ring_step(3, 4)
+    along_lines(3, 4)
+    pass_on(1, 2)
+    pass_on(0, 3)
+    pass_on(0, 4)
     pass_on(1, 3)
-    ring_step(2, 4)
-    along_lines(2, 3)
-    along_lines(2, 4)
-    pass_on(3, 1)
-    ring_step(3, 4)
-    along_lines(3, 2)
-    along_lines(3, 3)
-    along_lines(3, 4)
-    pass_on(0, 4)
+    pass_on(1, 4)
+    gather_stream()
     pass_on(2, 2)
-    gather_stream()
+    pass_on(2, 3)
     windows()
-    pass_on(1, 4)
+    pass_on(2, 4)
     stream_ready()
+    pass_on(3, 2)
     project_0()
-    pass_on(2, 3)
-    pass_on(2, 4)
-    pass_on(3, 2)
-    project_1()
     pass_on(3, 3)
     pass_on(3, 4)
+    project_1()
     settle()
     project_2()
     project_3()

time: 64.1 us -> 62.9 us (0.981)
  Pallas kernels: 62.5 us -> 61.4 us
    pallas_call x1, Pallas kernels: 62.5 us -> 61.4 us  [per_device(): pl.pallas_call(kernel, out_shape=pltpu.VMEM(stream.shape, bf16), in_specs...]
where the time goes in v4:
time: 62.9 us; the launch traced here: 62.1 us
  Pallas kernels  61.4 us (98%)
  local copies, waits for them, and re-layouts  0.71 us (1%)
    pallas_call x1, Pallas kernels, per_device(): pl.pallas_call(kernel, out_shape=pltpu.VMEM(stream.shape, bf16), in_specs...  61.4 us

profile of v4, /device:TPU:8, one launch (start us, length us, event | category | flops | bytes accessed | tf_op | source)
XLA Modules:
  0.0 62.1 jit_solution(8928409795509385870)
XLA Ops:
  0.0 61.4 %shard_map.55 = bf16[128,1024]{1,0:T(8,128)(2,1)S(1)} custom-call(bf16[128,1024]{1,0:T(8,128)(2,1)} %stream_hbm.1, f32[2,128]{1,0:T(2,128)} %gain_hbm.1, bf16[2,64,128]{2,1,0:T(8,128)(2,1)} %bitcast.2, bf16[2,64,128]{2,1,0:T(8,128)(2,1)} %out_w.1, s32[8,128]{1,0:T(8,128)} %bitcast.3), custom_call_target="tpu_custom_call" | custom-call | tf_op jit(solution)/shard_map/pallas_call | solution.py:558
  61.4 0.7 %copy.7 = bf16[128,1024]{1,0:T(8,128)(2,1)} copy(bf16[128,1024]{1,0:T(8,128)(2,1)S(1)} %shard_map.55) | data formatting | bytes 524288

commit v5 on v4

--- a/solution.py
+++ b/solution.py
@@ -83,8 +83,10 @@
         return (value + by + size) % size
 
     sibling = (sp, z * 2 + 1 - core)
-    has_next = jnp.logical_and(z == NZ - 1, sp < NY * NX - 1)
-    has_edge = jnp.logical_and(z == 0, sp > 0)
+    has_next = jnp.logical_or(z < NZ - 1, sp < NY * NX - 1)
+    has_edge = jnp.logical_or(z > 0, sp > 0)
+    next_sp, next_z = sp + z // (NZ - 1), (z + 1) % NZ
+    last_sp, last_z = sp - (NZ - 1 - z) // (NZ - 1), (z + NZ - 1) % NZ
 
     def copy(src, dst, send, recv, device):
         return pltpu.make_async_remote_copy(
@@ -102,15 +104,15 @@
     for peer in peers:
         pl.semaphore_signal(barrier, inc=1, device_id=peer, device_id_type=MESH)
 
-    @pl.when(has_next)
-    def _():
-        pl.semaphore_signal(barrier, inc=1, device_id=(sp + 1, core), device_id_type=MESH)
-
-    @pl.when(has_edge)
-    def _():
-        pl.semaphore_signal(
-            barrier, inc=1, device_id=(sp - 1, (NZ - 1) * 2 + core), device_id_type=MESH
-        )
+    for c in (core, 1 - core):
+
+        @pl.when(has_next)
+        def _(c=c):
+            pl.semaphore_signal(barrier, inc=1, device_id=(next_sp, next_z * 2 + c), device_id_type=MESH)
+
+        @pl.when(has_edge)
+        def _(c=c):
+            pl.semaphore_signal(barrier, inc=1, device_id=(last_sp, last_z * 2 + c), device_id_type=MESH)
 
     loads = []
     for layer in range(LAYERS):
@@ -134,7 +136,7 @@
         own_gain[...] = jnp.zeros_like(own_gain)
         own_gain[0:LAYERS, :] = gain[...]
 
-    extra = jnp.logical_or(has_next, has_edge).astype(jnp.int32)
+    extra = 2 * has_next.astype(jnp.int32) + 2 * has_edge.astype(jnp.int32)
     pl.semaphore_wait(barrier, len(peers) + extra)
 
     def send_plane(group):
@@ -213,73 +215,47 @@
         target = at(y, x, zz)
         copy(own_gain, gains.at[core, z], gain_send, gain_recv, target).start()
 
-        @pl.when(zz == 0)
-        def _():
-            copy(
-                turned.at[0:TOK, :], taken.at[core, z, HALO:ROWS, :], take_send, take_recv, target
-            ).start()
-
-        @pl.when(zz > 0)
-        def _():
-            first = pl.multiple_of(jnp.maximum(zz * TOK - HALO, 0), 32)
-            copy(
-                turned.at[pl.ds(first, ROWS), :], taken.at[core, z], take_send, take_recv, target
-            ).start()
+        block = turned.at[pl.ds(pl.multiple_of(zz * TOK, TOK), TOK), :]
+        copy(block, taken.at[core, z, HALO:ROWS, :], take_send, take_recv, target).start()
 
     def gather_stream():
         gains[core, z] = own_gain[...]
 
-        @pl.when(z == 0)
-        def _():
-            taken[core, z, HALO:ROWS, :] = turned[0:TOK, :]
-
-        @pl.when(z > 0)
-        def _():
-            first = pl.multiple_of(jnp.maximum(z * TOK - HALO, 0), 32)
-            taken[core, z] = turned[pl.ds(first, ROWS), :]
-
+        taken[core, z, HALO:ROWS, :] = turned[pl.ds(pl.multiple_of(z * TOK, TOK), TOK), :]
         drain(gains.at[0, 0:7], gain_recv)
-
-        @pl.when(z == 0)
-        def _():
-            drain(taken.at[0, 0:7, HALO:ROWS, :], take_recv)
-
-        @pl.when(z > 0)
-        def _():
-            drain(taken.at[0, 0:7], take_recv)
-
-        to_next = copy(
-            taken.at[core, :, TOK:ROWS, :],
-            taken.at[core, :, 0:HALO, :],
-            edge_send.at[0],
-            edge_recv.at[0],
-            (sp + 1, core),
+        drain(taken.at[0, 0:7, HALO:ROWS, :], take_recv)
+
+        @pl.when(has_next)
+        def _():
+            for one in edges(core):
+                one.start()
+
+        half = taken.at[core, :, HALO:ROWS, :]
+        copy(half, half, pair_send.at[0], pair_recv.at[0], sibling).start()
+        half = gains.at[core]
+        copy(half, half, pair_send.at[1], pair_recv.at[1], sibling).start()
+
+    def edges(c):
+        last, first = taken.at[c, :, TOK:ROWS, :], taken.at[c, :, 0:HALO, :]
+        return (
+            copy(last, first, edge_send.at[0], edge_recv.at[0], (next_sp, next_z * 2 + core)),
+            copy(last, first, edge_send.at[1], edge_recv.at[1], (next_sp, next_z * 2 + 1 - core)),
+            copy(docs, edge_docs, edge_send.at[2], edge_recv.at[2], (next_sp, next_z * 2 + core)),
         )
-        docs_next = copy(docs, edge_docs, edge_send.at[1], edge_recv.at[1], (sp + 1, core))
-
-        @pl.when(has_next)
-        def _():
-            to_next.start()
-            docs_next.start()
-            to_next.wait_send()
-            docs_next.wait_send()
-
+
+    def windows():
         @pl.when(has_edge)
         def _():
-            to_next.wait_recv()
-            docs_next.wait_recv()
+            same, other, papers = edges(core)
+            same.wait_recv()
+            other.wait_recv()
+            papers.wait_recv()
 
         @pl.when(jnp.logical_and(z == 0, sp == 0))
         def _():
-            taken[core, :, 0:HALO, :] = jnp.zeros((NZ, HALO, LANES), jnp.bfloat16)
+            taken[:, :, 0:HALO, :] = jnp.zeros((2, NZ, HALO, LANES), jnp.bfloat16)
             edge_docs[...] = jnp.full(edge_docs.shape, -1, jnp.int32)
 
-        mine = taken.at[core]
-        copy(mine, mine, pair_send.at[0], pair_recv.at[0], sibling).start()
-        mine = gains.at[core]
-        copy(mine, mine, pair_send.at[1], pair_recv.at[1], sibling).start()
-
-    def windows():
         own = docs[pl.ds(z, 1), :].astype(jnp.float32)
         inside = docs[pl.ds(turn(z, -1, NZ), 1), :].astype(jnp.float32)
 
@@ -311,7 +287,7 @@
         return k % 2, k // 2
 
     def stream_in():
-        pltpu.make_async_copy(taken.at[0], taken.at[0], pair_recv.at[0]).wait()
+        drain(taken.at[0, :, HALO:ROWS, :], pair_recv.at[0])
         pltpu.make_async_copy(gains.at[0], gains.at[0], pair_recv.at[1]).wait()
         for k in range(16):
             residual[block_of(k)] = taken[block_of(k)].astype(jnp.float32)
@@ -509,12 +485,12 @@
     pass_on(1, 2)
     pass_on(0, 3)
     pass_on(0, 4)
+    gather_stream()
     pass_on(1, 3)
     pass_on(1, 4)
-    gather_stream()
     pass_on(2, 2)
+    windows()
     pass_on(2, 3)
-    windows()
     pass_on(2, 4)
     stream_ready()
     pass_on(3, 2)
@@ -534,15 +510,14 @@
         drain(weights.at[w, 0:3], line_send.at[w])
     drain(gains.at[0, 0:7], gain_send)
 
-    @pl.when(z == 0)
+    drain(taken.at[0, 0:7, HALO:ROWS, :], take_send)
+
+    @pl.when(has_next)
     def _():
-        drain(taken.at[0, 0:7], take_send)
-
-    @pl.when(z > 0)
-    def _():
-        drain(taken.at[0, :, 0 : ROWS - 24, :], take_send)
-
-    pltpu.make_async_copy(taken.at[0], taken.at[0], pair_send.at[0]).wait()
+        for one in edges(core):
+            one.wait_send()
+
+    drain(taken.at[0, :, HALO:ROWS, :], pair_send.at[0])
     pltpu.make_async_copy(gains.at[0], gains.at[0], pair_send.at[1]).wait()
     for q in range(4):
         pair = pl.ds(2 * q, 2)
@@ -591,8 +566,8 @@
             dma,
             dma,
             dma,
-            dma((2,)),
-            dma((2,)),
+            dma((3,)),
+            dma((3,)),
             dma((2,)),
             dma((2,)),
             dma((4,)),

time: 62.9 us -> 62.7 us (level)
  the two profiles are of different devices: /device:TPU:8 before, /device:TPU:32 now
where the time goes in v5:
time: 62.7 us; the launch traced here: 62.5 us
  Pallas kernels  61.8 us (99%)
  local copies, waits for them, and re-layouts  0.71 us (1%)
    pallas_call x1, Pallas kernels, per_device(): pl.pallas_call(kernel, out_shape=pltpu.VMEM(stream.shape, bf16), in_specs...  61.8 us

profile of v5, /device:TPU:32, one launch (start us, length us, event | category | flops | bytes accessed | tf_op | source)
XLA Modules:
  0.0 62.5 jit_solution(17437704394930555533)
XLA Ops:
  0.0 61.8 %shard_map.55 = bf16[128,1024]{1,0:T(8,128)(2,1)S(1)} custom-call(bf16[128,1024]{1,0:T(8,128)(2,1)} %stream_hbm.1, f32[2,128]{1,0:T(2,128)} %gain_hbm.1, bf16[2,64,128]{2,1,0:T(8,128)(2,1)} %bitcast.2, bf16[2,64,128]{2,1,0:T(8,128)(2,1)} %out_w.1, s32[8,128]{1,0:T(8,128)} %bitcast.3), custom_call_target="tpu_custom_call" | custom-call | tf_op jit(solution)/shard_map/pallas_call | solution.py:533
  61.8 0.7 %copy.7 = bf16[128,1024]{1,0:T(8,128)(2,1)} copy(bf16[128,1024]{1,0:T(8,128)(2,1)S(1)} %shard_map.55) | data formatting | bytes 524288
